TPU v7x, 32 devices: a whole 2x2x4 slice. The times are simulated.
32 devices in a mesh: sp: 8 (over z, core), tp: 4 (over y, x).
Axes of the slice: x: 2, y: 2, z: 4, core: 2. Of those that a mesh axis runs over, the one named last changes fastest.
Arguments:
- layer_input: bfloat16 [8192, 4096], P('sp', 'tp'), may hold values from -6 to 6
- key_weight: bfloat16 [4096, 4096], P(None, 'tp'), may hold values from -0.09375 to 0.09375
- value_weight: bfloat16 [4096, 4096], P(None, 'tp'), may hold values from -0.09375 to 0.09375
- decay_exponent: float32 [32], P('tp'), may hold values from -0.077 to -0.00016845703, as said below
- query_new: bfloat16 [2, 4096], P(None, 'tp'), may hold values from -6 to 6
- key_new: bfloat16 [2, 4096], P(None, 'tp'), may hold values from -6 to 6
- value_new: bfloat16 [2, 4096], P(None, 'tp'), may hold values from -6 to 6
- norm_gain: float32 [4096], P('tp'), may hold values from 0.1 to 1.9
Outputs:
- state_cache: bfloat16 [2, 32, 128, 128], P(None, 'tp', 'sp')
- first_read: bfloat16 [2, 4096], P(None, 'tp')
Inputs may be any that keep to these rules, and one draw needn't show every extreme that they name: decay_exponent is negative.
All inputs are finite; a program needn't handle non-finite values.
Results may differ from a plain program's by a relative error of at most 0.011.
Values may be sent and summed in bfloat16 or wider, within the bound.
A program may use at most 64 MiB of HBM per device.

v0:
```python
import jax
import jax.numpy as jnp
from jax import lax
from jax.sharding import PartitionSpec as P

SEQS = 2


def rotate(projected, position):
    half_width = projected.shape[-1] // 2
    inverse = 1.0 / 10000.0 ** jnp.linspace(0.0, 1.0, half_width, dtype=jnp.float32)
    angle = position[:, None] * inverse[None, :]
    cosine = jnp.cos(angle)[:, None, :]
    sine = jnp.sin(angle)[:, None, :]
    first = projected[..., :half_width]
    second = projected[..., half_width:]
    return jnp.concatenate(
        [first * cosine - second * sine, first * sine + second * cosine], axis=-1
    )


def on_device(
    layer_input, key_weight, value_weight, decay_exponent, query_new, key_new, value_new, norm_gain
):
    tok_count = layer_input.shape[0]
    head_local = decay_exponent.shape[0]
    key_width = key_weight.shape[1] // head_local
    value_width = value_weight.shape[1] // head_local
    seq_span = lax.axis_size("sp") // SEQS
    seq_length = tok_count * seq_span
    sp_place = lax.axis_index("sp")
    feature_block = lax.all_gather(layer_input, "tp", axis=1, tiled=True)
    key_proj = jnp.dot(feature_block, key_weight, preferred_element_type=jnp.float32)
    value_proj = jnp.dot(feature_block, value_weight, preferred_element_type=jnp.float32)
    position = (sp_place % seq_span * tok_count + jnp.arange(tok_count, dtype=jnp.int32)).astype(
        jnp.float32
    )
    keys = (
        rotate(key_proj.reshape(tok_count, head_local, key_width), position) * key_width ** (-0.5)
    ).astype(jnp.bfloat16)
    values = value_proj.astype(jnp.bfloat16).reshape(tok_count, head_local, value_width)
    distance = seq_length - 1.0 - position
    weighting = jnp.exp(decay_exponent[None, :] * distance[:, None])
    weighted = (keys.astype(jnp.float32) * weighting[:, :, None]).astype(jnp.bfloat16)
    local_state = jnp.einsum("thd,the->hde", weighted, values, preferred_element_type=jnp.float32)
    member = (jnp.arange(SEQS, dtype=jnp.int32) == sp_place // seq_span).astype(jnp.float32)
    state_terms = member[:, None, None, None] * local_state[None]
    final_rows = lax.psum_scatter(state_terms, "sp", scatter_dimension=2, tiled=True)
    state_cache = final_rows.astype(jnp.bfloat16)
    queries = query_new.astype(jnp.float32).reshape(SEQS, head_local, key_width)
    partial_read = jnp.einsum(
        "shd,shde->she", queries, state_terms, precision=lax.Precision.HIGHEST
    )
    carried = lax.psum(partial_read, "sp")
    keys_next = key_new.astype(jnp.float32).reshape(SEQS, head_local, key_width)
    values_next = value_new.astype(jnp.float32).reshape(SEQS, head_local, value_width)
    own_term = jnp.sum(queries * keys_next, axis=2)[:, :, None] * values_next
    mixed = jnp.exp(decay_exponent)[None, :, None] * carried + own_term
    normed = mixed * lax.rsqrt(jnp.mean(mixed * mixed, axis=2, keepdims=True) + 1e-06)
    normed = normed * norm_gain.reshape(head_local, value_width)[None, :, :]
    return (state_cache, normed.reshape(SEQS, head_local * value_width).astype(jnp.bfloat16))


def solution(mesh):
    in_specs = (
        P("sp", "tp"),
        P(None, "tp"),
        P(None, "tp"),
        P("tp"),
        P(None, "tp"),
        P(None, "tp"),
        P(None, "tp"),
        P("tp"),
    )
    out_specs = (P(None, "tp", "sp", None), P(None, "tp"))
    return jax.shard_map(
        on_device, mesh=mesh, in_specs=in_specs, out_specs=out_specs, check_vma=False
    )
```

profile of v0, /device:TPU:0, one launch (start us, length us, event | category | flops | bytes accessed | tf_op | source)
XLA Modules:
  0.0 171.2 jit_solution(11473532928308546510)
XLA Ops:
  7.2 0.0 all-gather.2.cloned.1.call-start
  7.2 0.7 all-gather.2.cloned.1.call-update
  7.9 0.0 reduce-scatter.2.cloned.1.call-start
  8.0 0.1 fusion.12
  8.1 0.7 multiply_exponential_fusion
  8.8 1.0 multiply_cosine_fusion
  9.8 90.2 %all-gather.2.cloned.1.call-done = bf16[1024,4096]{1,0:T(8,128)(2,1)} async-done(((bf16[1024,1024]{1,0:T(8,128)(2,1)}), bf16[1024,4096]{1,0:T(8,128)(2,1)}) %all-gather.2.cloned.1.call-update) | async-done | bytes 8388624 | tf_op jit(solution)/shard_map/all_gather | solution.py:32
  100.1 13.2 %fusion.15 = f32[1024,1024]{0,1:T(8,128)S(1)} fusion(bf16[1024,4096]{1,0:T(8,128)(2,1)} %all-gather.2.cloned.1.call-done, bf16[4096,1024]{1,0:T(8,128)(2,1)} %param.9), kind=kOutput, calls=%fused_computation.35 | convolution fusion | flops 8589934592 | bytes 20971520 | tf_op jit(solution)/shard_map/dot_general | solution.py:33
  113.3 1.0 multiply_subtract_fusion
  114.3 13.8 %convolution_convert_fusion = bf16[1024,1024]{0,1:T(8,128)(2,1)S(1)} fusion(bf16[1024,4096]{1,0:T(8,128)(2,1)} %all-gather.2.cloned.1.call-done, bf16[4096,1024]{1,0:T(8,128)(2,1)} %param.10), kind=kOutput, calls=%fused_computation.9 | convolution fusion | flops 8590983168 | bytes 18874368 | tf_op jit(solution)/shard_map/dot_general | solution.py:34
  128.1 0.0 copy-start.4
  128.1 0.0 copy-start
  128.1 0.0 copy-start.1
  128.1 0.0 copy-start.3
  128.1 0.0 copy-start.2
  128.1 0.7 fusion.2
  128.9 1.1 broadcast_multiply_fusion
  130.0 0.0 reduce-scatter.2.cloned.1.call-update
  130.0 0.0 copy-done.4
  130.0 0.0 copy-done
  130.1 0.0 copy-done.1
  130.1 0.0 copy-done.3
  130.1 0.7 fusion.8
  130.8 16.6 %psum.7 = f32[2,8,128]{2,1,0:T(8,128)S(1)} all-reduce(f32[2,8,128]{2,1,0:T(8,128)S(1)} %bitcast.29), channel_id=1, replica_groups=mesh['sp'=8,'tp'=4] {'sp'}, use_global_device_ids=true, to_apply=%region_1.2 | all-reduce | flops 2048 | bytes 16384 | tf_op jit(solution)/shard_map/psum | solution.py:54
  147.4 0.2 multiply_reduce_fusion
  147.6 0.0 copy-done.2
  147.6 0.1 fusion.11
  147.6 0.6 copy.26
  148.2 14.6 %reduce-scatter.2.cloned.1.call-done = f32[2,8,16,128]{3,2,1,0:T(8,128)} async-done(((f32[2,8,128,128]{3,2,1,0:T(8,128)}), f32[2,8,16,128]{3,2,1,0:T(8,128)}) %reduce-scatter.2.cloned.1.call-update) | async-done | bytes 131088 | tf_op jit(solution)/shard_map/reduce_scatter | solution.py:48
  162.8 1.5 convert_element_type.51
  (9 shorter events, 0.1 us)
Async XLA Ops:
  7.2 92.9 %all-gather.2.cloned.1.call-start = ((), (), s32[]{:S(2)}) async-start(), calls=%async_computation.1 | async-start | bytes 10485760 | tf_op jit(solution)/shard_map/all_gather | solution.py:32
  7.9 154.9 %reduce-scatter.2.cloned.1.call-start = ((), (), s32[]{:S(2)}) async-start(), calls=%async_computation.2 | async-start | bytes 1179648 | tf_op jit(solution)/shard_map/reduce_scatter | solution.py:48
  128.1 1.9 %copy-start.4 = (f32[8]{0:T(128)S(1)}, f32[8]{0:T(128)}, u32[]{:S(2)}) copy-start(f32[8]{0:T(128)} %param.11) | copy-start | bytes 100
  128.1 2.0 %copy-start = (bf16[2,1024]{1,0:T(2,128)(2,1)S(1)}, bf16[2,1024]{1,0:T(2,128)(2,1)}, u32[]{:S(2)}) copy-start(bf16[2,1024]{1,0:T(2,128)(2,1)} %param.12) | copy-start | bytes 12292
  128.1 2.0 %copy-start.1 = (bf16[2,1024]{1,0:T(2,128)(2,1)S(1)}, bf16[2,1024]{1,0:T(2,128)(2,1)}, u32[]{:S(2)}) copy-start(bf16[2,1024]{1,0:T(2,128)(2,1)} %param.14) | copy-start | bytes 12292
  128.1 2.0 %copy-start.3 = (bf16[2,1024]{1,0:T(2,128)(2,1)S(1)}, bf16[2,1024]{1,0:T(2,128)(2,1)}, u32[]{:S(2)}) copy-start(bf16[2,1024]{1,0:T(2,128)(2,1)} %param.13) | copy-start | bytes 12292
  128.1 19.4 %copy-start.2 = (f32[1024]{0:T(1024)S(1)}, f32[1024]{0:T(1024)}, u32[]{:S(2)}) copy-start(f32[1024]{0:T(1024)} %param.15) | copy-start | bytes 12292
Sparse Core Ops, SparseCore 0:
  9.8 90.1 all-gather.1
  130.1 32.6 reduce-scatter.1
where the time goes:
time: 171 us
  waiting for transfers between devices  106 us (62%)
  matrix products  28.4 us (17%)
  blocking collectives  16.6 us (10%)
  between operations  14.2 us (8%)
  other arithmetic  5.78 us (3%)
    all_gather x1, waiting for transfers between devices, on_device(): feature_block = lax.all_gather(layer_input, 'tp', axis=1, tiled=True)  90.2 us
    psum x1, blocking collectives, on_device(): carried = lax.psum(partial_read, 'sp')  16.6 us
    reduce_scatter x1, waiting for transfers between devices, on_device(): lax.psum_scatter(state_terms, 'sp', scatter_dimension=2, tiled=True)  14.6 us
    dot_general x1, matrix products, on_device(): jnp.dot(feature_block, value_weight, preferred_element_type=jnp.float32)  13.8 us
    dot_general x1, matrix products, on_device(): jnp.dot(feature_block, key_weight, preferred_element_type=jnp.float32)  13.2 us
  transfers between devices with their start and end apart: 2, of which 2 were waited for; matrix products, arithmetic and copies ran while one was open for 2% of the time, Pallas kernels for 0%

commit v1 on v0

v1 whole, which is shorter than its diff:
```python
import functools
import math

import jax
import jax.numpy as jnp
import numpy as np
from jax import lax
from jax.experimental import pallas as pl
from jax.experimental.pallas import tpu as pltpu
from jax.sharding import PartitionSpec as P

SEQS = 2
CHUNKS = 4
MESH = pl.DeviceIdType.MESH
F32 = jnp.float32
BF16 = jnp.bfloat16


def gather_kernel(
    side, seq_span, chunks,
    decay_ref, inv_ref, x_ref, wk_ref, wv_ref,
    state_ref,
    gx, wk, wv, cosine, sine, acc_k, acc_v,
    send_sem, recv_sem, local_sem,
):
    tokens, feats = x_ref.shape
    rows = tokens // chunks
    half = rows // 2
    heads, width, vwidth = state_ref.shape
    pair = 2 if heads % 2 == 0 else 1
    me = lax.axis_index("tp")
    my_y, my_x = me // side, lax.rem(me, side)
    sp_place = lax.axis_index("sp")

    def x_peer(d):
        return my_y * side + lax.rem(my_x + d, side)

    def y_peer(d):
        return lax.rem(my_y + d, side) * side + my_x

    x_peers = [x_peer(d) for d in range(1, side)]
    y_peers = [y_peer(d) for d in range(1, side)]

    local = [
        pltpu.make_async_copy(x_ref, gx.at[me], local_sem.at[0]),
        pltpu.make_async_copy(wk_ref, wk, local_sem.at[1]),
        pltpu.make_async_copy(wv_ref, wv, local_sem.at[2]),
    ]
    for copy in local:
        copy.start()

    barrier = pltpu.get_barrier_semaphore()
    for peer in x_peers + y_peers:
        pl.semaphore_signal(barrier, inc=1, device_id={"tp": peer}, device_id_type=MESH)
    pl.semaphore_wait(barrier, 2 * (side - 1))

    def span(c, part):
        return pl.ds(pl.multiple_of(c * rows + part * half, half), half)

    def remote(c, slot, block, part, target, from_input):
        where = span(c, part)
        return pltpu.make_async_remote_copy(
            src_ref=x_ref.at[where] if from_input else gx.at[block, where],
            dst_ref=gx.at[block, where],
            send_sem=send_sem.at[c, slot],
            recv_sem=recv_sem.at[c, block, part],
            device_id={"tp": target},
            device_id_type=MESH,
        )

    def own_copies(c):
        out, slot = [], 0
        for first in (True, False):
            for part, peers in ((0, x_peers), (1, y_peers)):
                for peer in peers:
                    out.append(remote(c, slot, me, part if first else 1 - part, peer, True))
                    slot += 1
        return out

    def relay_copies(c):
        out, slot = [], 4 * (side - 1)
        for part, sources, peers in ((0, x_peers, y_peers), (1, y_peers, x_peers)):
            for source in sources:
                for peer in peers:
                    out.append(remote(c, slot, source, part, peer, False))
                    slot += 1
        return out

    def arrived(c, block, part):
        remote(c, 0, block, part, x_peers[0], False).wait_recv()

    late_blocks = [
        lax.rem(my_y + dy, side) * side + lax.rem(my_x + dx, side)
        for dy in range(1, side)
        for dx in range(1, side)
    ]

    def wait_early(c):
        for block in x_peers + y_peers:
            for part in range(2):
                arrived(c, block, part)

    def wait_late(c):
        for block in late_blocks:
            for part in range(2):
                arrived(c, block, part)

    def start_all(copies):
        for copy in copies:
            copy.start()

    start_all(own_copies(0))
    if chunks > 1:
        start_all(own_copies(1))

    state_ref[...] = jnp.zeros_like(state_ref)
    base = lax.rem(sp_place, seq_span) * tokens

    def table(c, _):
        at = pl.ds(pl.multiple_of(c * half, half), half)
        place = (base + c * half + lax.broadcasted_iota(jnp.int32, (half, width), 0)).astype(F32)
        angle = place * inv_ref[...]
        low = lax.broadcasted_iota(jnp.int32, (half, width), 1) < width // 2
        sin = jnp.sin(angle)
        cosine[at, :] = jnp.cos(angle)
        sine[at, :] = jnp.where(low, -sin, sin)
        return 0

    lax.fori_loop(0, 2 * chunks, table, 0)
    for copy in local:
        copy.wait()

    def partial(c, blocks, w, cols):
        at = pl.ds(pl.multiple_of(c * rows, rows), rows)
        total = None
        for block in blocks:
            depth = pl.ds(pl.multiple_of(block * feats, feats), feats)
            term = jnp.dot(gx[block, at, :], w[depth, cols], preferred_element_type=F32)
            total = term if total is None else total + term
        return total

    early_blocks = [me] + x_peers + y_peers

    def finish(c, blocks, carry):
        at = pl.ds(pl.multiple_of(c * rows, rows), rows)
        distance = (seq_span * tokens - 1 - base - c * rows) - lax.broadcasted_iota(
            jnp.int32, (rows, width), 0
        )
        distance = distance.astype(F32)

        def step(g, _):
            kcols = pl.ds(pl.multiple_of(g * pair * width, pair * width), pair * width)
            vcols = pl.ds(pl.multiple_of(g * pair * vwidth, pair * vwidth), pair * vwidth)
            k = partial(c, blocks, wk, kcols)
            v = partial(c, blocks, wv, vcols)
            if carry:
                k = k + acc_k[:, kcols]
                v = v + acc_v[:, vcols]
            v = v.astype(BF16)
            for j in range(pair):
                kh = k[:, j * width:(j + 1) * width]
                turned = kh * cosine[at, :] + pltpu.roll(kh, width // 2, 1) * sine[at, :]
                keys = (turned * width ** (-0.5)).astype(BF16).astype(F32)
                weighted = (keys * jnp.exp(decay_ref[g * pair + j] * distance)).astype(BF16)
                state_ref[g * pair + j] += lax.dot_general(
                    weighted, v[:, j * vwidth:(j + 1) * vwidth],
                    (((0,), (0,)), ((), ())), preferred_element_type=F32,
                )
            return 0

        lax.fori_loop(0, heads // pair, step, 0)

    def round_trip(c, _):
        wait_early(c)
        start_all(relay_copies(c))

        @pl.when(c + 2 < chunks)
        def _():
            start_all(own_copies(c + 2))

        @pl.when(c > 0)
        def _():
            wait_late(c - 1)
            finish(c - 1, early_blocks + late_blocks, False)

        return 0

    lax.fori_loop(0, chunks, round_trip, 0)
    last = chunks - 1

    def early(g, _):
        kcols = pl.ds(pl.multiple_of(g * pair * width, pair * width), pair * width)
        vcols = pl.ds(pl.multiple_of(g * pair * vwidth, pair * vwidth), pair * vwidth)
        acc_k[:, kcols] = partial(last, early_blocks, wk, kcols)
        acc_v[:, vcols] = partial(last, early_blocks, wv, vcols)
        return 0

    lax.fori_loop(0, heads // pair, early, 0)
    wait_late(last)
    finish(last, late_blocks, True)

    def drain(c, _):
        for copy in own_copies(c) + relay_copies(c):
            copy.wait_send()
        return 0

    lax.fori_loop(0, chunks, drain, 0)


def local_states(layer_input, key_weight, value_weight, decay_exponent, seq_span):
    tokens, feats = layer_input.shape
    depth = key_weight.shape[0]
    parts = lax.axis_size("tp")
    side = math.isqrt(parts)
    heads = decay_exponent.shape[0]
    width = key_weight.shape[1] // heads
    vwidth = value_weight.shape[1] // heads
    steps = np.linspace(0.0, 1.0, width // 2, dtype=np.float32)
    inverse = (np.float32(1.0) / np.power(np.float32(10000.0), steps)).astype(np.float32)
    inverse = jnp.asarray(np.concatenate([inverse, inverse])[None, :])
    sends = 4 * (side - 1) + 2 * (side - 1) ** 2
    anywhere = pl.BlockSpec(memory_space=pl.ANY)
    vmem = pl.BlockSpec(memory_space=pltpu.VMEM)
    rows = tokens // CHUNKS
    return pl.pallas_call(
        functools.partial(gather_kernel, side, seq_span, CHUNKS),
        out_shape=jax.ShapeDtypeStruct((heads, width, vwidth), F32),
        in_specs=[pl.BlockSpec(memory_space=pltpu.SMEM), vmem, anywhere, anywhere, anywhere],
        out_specs=vmem,
        scratch_shapes=[
            pltpu.VMEM((parts, tokens, feats), BF16),
            pltpu.VMEM(key_weight.shape, BF16),
            pltpu.VMEM(value_weight.shape, BF16),
            pltpu.VMEM((tokens, width), F32),
            pltpu.VMEM((tokens, width), F32),
            pltpu.VMEM((rows, heads * width), F32),
            pltpu.VMEM((rows, heads * vwidth), F32),
            pltpu.SemaphoreType.DMA((CHUNKS, sends)),
            pltpu.SemaphoreType.DMA((CHUNKS, parts, 2)),
            pltpu.SemaphoreType.DMA((3,)),
        ],
        compiler_params=pltpu.CompilerParams(
            collective_id=0, has_side_effects=True, vmem_limit_bytes=56 * 1024 * 1024
        ),
    )(decay_exponent, inverse, layer_input, key_weight, value_weight)


def on_device(
    layer_input, key_weight, value_weight, decay_exponent, query_new, key_new, value_new, norm_gain
):
    head_local = decay_exponent.shape[0]
    key_width = key_weight.shape[1] // head_local
    value_width = value_weight.shape[1] // head_local
    seq_span = lax.axis_size("sp") // SEQS
    sp_place = lax.axis_index("sp")
    local_state = local_states(layer_input, key_weight, value_weight, decay_exponent, seq_span)
    member = (jnp.arange(SEQS, dtype=jnp.int32) == sp_place // seq_span).astype(jnp.float32)
    state_terms = member[:, None, None, None] * local_state[None]
    final_rows = lax.psum_scatter(state_terms, "sp", scatter_dimension=2, tiled=True)
    state_cache = final_rows.astype(jnp.bfloat16)
    queries = query_new.astype(jnp.float32).reshape(SEQS, head_local, key_width)
    partial_read = jnp.einsum(
        "shd,shde->she", queries, state_terms, precision=lax.Precision.HIGHEST
    )
    carried = lax.psum(partial_read, "sp")
    keys_next = key_new.astype(jnp.float32).reshape(SEQS, head_local, key_width)
    values_next = value_new.astype(jnp.float32).reshape(SEQS, head_local, value_width)
    own_term = jnp.sum(queries * keys_next, axis=2)[:, :, None] * values_next
    mixed = jnp.exp(decay_exponent)[None, :, None] * carried + own_term
    normed = mixed * lax.rsqrt(jnp.mean(mixed * mixed, axis=2, keepdims=True) + 1e-06)
    normed = normed * norm_gain.reshape(head_local, value_width)[None, :, :]
    return (state_cache, normed.reshape(SEQS, head_local * value_width).astype(jnp.bfloat16))


def solution(mesh):
    in_specs = (
        P("sp", "tp"),
        P(None, "tp"),
        P(None, "tp"),
        P("tp"),
        P(None, "tp"),
        P(None, "tp"),
        P(None, "tp"),
        P("tp"),
    )
    out_specs = (P(None, "tp", "sp", None), P(None, "tp"))
    return jax.shard_map(
        on_device, mesh=mesh, in_specs=in_specs, out_specs=out_specs, check_vma=False
    )
```

time: 171 us -> 135 us (0.79)
  waiting for transfers between devices: 106 us -> 15.5 us
  Pallas kernels: 0 us -> 83.6 us
  matrix products: 28.4 us -> 1.72 us
  other arithmetic: 5.78 us -> 4.01 us
    all_gather x1 -> x0, waiting for transfers between devices: 90.2 us -> none  [on_device(): feature_block = lax.all_gather(layer_input, 'tp', axis=1, tiled=True)]
    pallas_call x0 -> x1, Pallas kernels: none -> 83.6 us  [local_states(): pl.pallas_call(functools.partial(gather_kernel, side, seq_span, CHUNKS),...]
    dot_general x3 -> x0, matrix products: 27.7 us -> none  [the longest x1 13.8 us: on_device(): jnp.dot(feature_block, value_weight, preferred_element_type=jnp.float32)]
  transfers between devices with their start and end apart: 2 -> 1, of which waited for: 2 -> 1; matrix products, arithmetic and copies ran while one was open for 2% -> 2% of each run, Pallas kernels for 0% -> 0%
where the time goes in v1:
time: 135 us
  Pallas kernels  83.6 us (62%)
  waiting for transfers between devices  15.5 us (11%)
  blocking collectives  15 us (11%)
  between operations  14.2 us (11%)
  other arithmetic  4.01 us (3%)
  matrix products  1.72 us (1%)
    pallas_call x1, Pallas kernels, local_states(): pl.pallas_call(functools.partial(gather_kernel, side, seq_span, CHUNKS),...  83.6 us
    reduce_scatter x1, waiting for transfers between devices, on_device(): lax.psum_scatter(state_terms, 'sp', scatter_dimension=2, tiled=True)  15.5 us
    psum x1, blocking collectives, on_device(): carried = lax.psum(partial_read, 'sp')  15 us
  transfers between devices with their start and end apart: 1, of which 1 were waited for; matrix products, arithmetic and copies ran while one was open for 2% of the time, Pallas kernels for 0%

profile of v1, /device:TPU:0, one launch (start us, length us, event | category | flops | bytes accessed | tf_op | source)
XLA Modules:
  0.0 134.7 jit_solution(17429130168309870691)
XLA Ops:
  7.2 0.0 reduce-scatter.2.cloned.1.call-start
  7.2 0.0 copy-start.4
  7.2 0.0 copy-start
  7.3 0.0 copy-start.1
  7.3 0.0 copy-start.3
  7.3 0.0 copy-start.2
  7.3 83.6 %shard_map.104 = f32[8,128,128]{2,1,0:T(8,128)} custom-call(f32[8]{0:T(128)} %decay_ref.1, f32[1,128]{1,0:T(1,128)} %constant.31.clone.inv_ref, bf16[1024,1024]{1,0:T(8,128)(2,1)} %x_ref.1, bf16[4096,1024]{1,0:T(8,128)(2,1)} %wk_ref.1, bf16[4096,1024]{1,0:T(8,128)(2,1)} %wv_ref.1), custom_call_target="tpu_custom_call" | custom-call | tf_op jit(solution)/shard_map/pallas_call | solution.py:225
  90.9 2.2 %broadcast_multiply_fusion = f32[2,8,128,128]{3,2,1,0:T(8,128)} fusion(f32[8,128,128]{2,1,0:T(8,128)} %shard_map.104, f32[2]{0:T(128)S(1)} %compare_convert_fusion), kind=kLoop, calls=%fused_computation.3 | loop fusion | flops 262144 | bytes 1572872 | tf_op jit(solution)/shard_map/mul | solution.py:258
  93.1 0.0 reduce-scatter.2.cloned.1.call-update
  93.1 0.0 copy-done.4
  93.1 0.0 copy-done
  93.2 1.7 %fusion.3 = f32[2,8,1,128]{3,2,1,0:T(1,128)S(1)} fusion(bf16[2,8,128,1]{2,3,1,0:T(2,128)(2,1)S(1)} %reshape.42, f32[8,128,128]{2,1,0:T(8,128)} %shard_map.104, f32[2]{0:T(128)S(1)} %compare_convert_fusion), kind=kOutput, calls=%fused_computation.4 | convolution fusion | flops 3407872 | bytes 536584 | tf_op jit(solution)/shard_map/shd,shde->she/dot_general | solution.py:262
  94.9 15.0 %psum.7 = f32[2,8,128]{2,1,0:T(8,128)S(1)} all-reduce(f32[2,8,128]{2,1,0:T(8,128)S(1)} %bitcast.21), channel_id=1, replica_groups=mesh['sp'=8,'tp'=4] {'sp'}, use_global_device_ids=true, to_apply=%region_1.2 | all-reduce | flops 2048 | bytes 16384 | tf_op jit(solution)/shard_map/psum | solution.py:265
  109.9 0.0 copy-done.1
  110.0 0.0 copy-done.3
  110.0 0.2 multiply_reduce_fusion
  110.2 0.0 copy-done.2
  110.2 0.1 fusion.6
  110.2 0.6 copy.25
  110.8 15.5 %reduce-scatter.2.cloned.1.call-done = f32[2,8,16,128]{3,2,1,0:T(8,128)} async-done(((f32[2,8,128,128]{3,2,1,0:T(8,128)}), f32[2,8,16,128]{3,2,1,0:T(8,128)}) %reduce-scatter.2.cloned.1.call-update) | async-done | bytes 131088 | tf_op jit(solution)/shard_map/reduce_scatter | solution.py:259
  126.3 1.5 %convert_element_type.24 = bf16[2,8,16,128]{3,2,1,0:T(8,128)(2,1)} convert(f32[2,8,16,128]{3,2,1,0:T(8,128)} %reduce-scatter.2.cloned.1.call-done) | non-fusion elementwise | flops 32768 | bytes 196608 | tf_op jit(solution)/shard_map/convert_element_type | solution.py:260
  (6 shorter events, 0.0 us)
Async XLA Ops:
  7.2 119.2 %reduce-scatter.2.cloned.1.call-start = ((), (), s32[]{:S(2)}) async-start(), calls=%async_computation.1 | async-start | bytes 1179648 | tf_op jit(solution)/shard_map/reduce_scatter | solution.py:259
  7.2 85.9 %copy-start.4 = (f32[8]{0:T(128)S(1)}, f32[8]{0:T(128)}, u32[]{:S(2)}) copy-start(f32[8]{0:T(128)} %decay_ref.1) | copy-start | bytes 100
  7.2 85.9 %copy-start = (bf16[2,1024]{1,0:T(2,128)(2,1)S(1)}, bf16[2,1024]{1,0:T(2,128)(2,1)}, u32[]{:S(2)}) copy-start(bf16[2,1024]{1,0:T(2,128)(2,1)} %param.13) | copy-start | bytes 12292
  7.3 102.7 %copy-start.1 = (bf16[2,1024]{1,0:T(2,128)(2,1)S(1)}, bf16[2,1024]{1,0:T(2,128)(2,1)}, u32[]{:S(2)}) copy-start(bf16[2,1024]{1,0:T(2,128)(2,1)} %param.15) | copy-start | bytes 12292
  7.3 102.7 %copy-start.3 = (bf16[2,1024]{1,0:T(2,128)(2,1)S(1)}, bf16[2,1024]{1,0:T(2,128)(2,1)}, u32[]{:S(2)}) copy-start(bf16[2,1024]{1,0:T(2,128)(2,1)} %param.14) | copy-start | bytes 12292
  7.3 102.9 %copy-start.2 = (f32[1024]{0:T(1024)S(1)}, f32[1024]{0:T(1024)}, u32[]{:S(2)}) copy-start(f32[1024]{0:T(1024)} %param.16) | copy-start | bytes 12292
Sparse Core Ops, SparseCore 0:
  93.2 33.0 reduce-scatter.1

commit v2 on v1

--- a/solution.py
+++ b/solution.py
@@ -18,10 +18,11 @@
 
 def gather_kernel(
     side, seq_span, chunks,
-    decay_ref, inv_ref, x_ref, wk_ref, wv_ref,
-    state_ref,
+    decay_ref, inv_ref, query_ref, key_ref, value_ref, gain_ref, x_ref, wk_ref, wv_ref,
+    cache_ref, first_ref,
     gx, wk, wv, cosine, sine, acc_k, acc_v,
-    send_sem, recv_sem, local_sem,
+    state_ref, query_wide, own_term, factor, staged, landed, read, reads,
+    send_sem, recv_sem, local_sem, state_send, state_recv, read_send, read_recv,
 ):
     tokens, feats = x_ref.shape
     rows = tokens // chunks
@@ -31,6 +32,10 @@
     me = lax.axis_index("tp")
     my_y, my_x = me // side, lax.rem(me, side)
     sp_place = lax.axis_index("sp")
+    sp_size = landed.shape[0]
+    kept = landed.shape[2]
+    groups = heads // pair
+    sp_peers = [lax.rem(sp_place + d, sp_size) for d in range(1, sp_size)]
 
     def x_peer(d):
         return my_y * side + lax.rem(my_x + d, side)
@@ -52,7 +57,9 @@
     barrier = pltpu.get_barrier_semaphore()
     for peer in x_peers + y_peers:
         pl.semaphore_signal(barrier, inc=1, device_id={"tp": peer}, device_id_type=MESH)
-    pl.semaphore_wait(barrier, 2 * (side - 1))
+    for peer in sp_peers:
+        pl.semaphore_signal(barrier, inc=1, device_id={"sp": peer}, device_id_type=MESH)
+    pl.semaphore_wait(barrier, 2 * (side - 1) + sp_size - 1)
 
     def span(c, part):
         return pl.ds(pl.multiple_of(c * rows + part * half, half), half)
@@ -127,6 +134,56 @@
         return 0
 
     lax.fori_loop(0, 2 * chunks, table, 0)
+
+    prompt = sp_place // seq_span
+    diagonal = lax.broadcasted_iota(jnp.int32, (width, width), 0) == lax.broadcasted_iota(
+        jnp.int32, (width, width), 1
+    )
+    ones = jnp.ones((width, vwidth), BF16)
+    queries = query_ref[...].astype(F32)
+    next_keys = key_ref[...].astype(F32)
+    next_values = value_ref[...].astype(F32)
+    for h in range(heads):
+        cols = slice(h * width, (h + 1) * width)
+        vcols = slice(h * vwidth, (h + 1) * vwidth)
+        mine = jnp.zeros((1, width), F32)
+        for s in range(SEQS):
+            mine = jnp.where(prompt == s, queries[s:s + 1, cols], mine)
+            score = jnp.sum(
+                queries[s:s + 1, cols] * next_keys[s:s + 1, cols], axis=1, keepdims=True
+            )
+            own_term[s, h] = score * next_values[s:s + 1, vcols]
+        spread = jnp.where(diagonal, jnp.broadcast_to(mine, (width, width)), 0.0).astype(BF16)
+        query_wide[h] = jnp.dot(spread, ones, preferred_element_type=F32)
+        factor[h] = jnp.exp(jnp.full((1, vwidth), decay_ref[h], F32))
+
+    def state_copies(g):
+        piece = pl.ds(g * pair, pair)
+        return [
+            pltpu.make_async_remote_copy(
+                src_ref=staged.at[peer, piece],
+                dst_ref=landed.at[sp_place, piece],
+                send_sem=state_send.at[g, d],
+                recv_sem=state_recv.at[g, sp_place],
+                device_id={"sp": peer},
+                device_id_type=MESH,
+            )
+            for d, peer in enumerate(sp_peers)
+        ]
+
+    def read_copies():
+        return [
+            pltpu.make_async_remote_copy(
+                src_ref=read,
+                dst_ref=reads.at[sp_place],
+                send_sem=read_send.at[d],
+                recv_sem=read_recv.at[sp_place],
+                device_id={"sp": peer},
+                device_id_type=MESH,
+            )
+            for d, peer in enumerate(sp_peers)
+        ]
+
     for copy in local:
         copy.wait()
 
@@ -166,9 +223,17 @@
                     weighted, v[:, j * vwidth:(j + 1) * vwidth],
                     (((0,), (0,)), ((), ())), preferred_element_type=F32,
                 )
+            if carry:
+                for j in range(pair):
+                    h = g * pair + j
+                    held = state_ref[h]
+                    for d in range(sp_size):
+                        staged[d, h] = held[d * kept:(d + 1) * kept, :].astype(BF16)
+                    read[h] = jnp.sum(query_wide[h] * held, axis=0, keepdims=True)
+                start_all(state_copies(g))
             return 0
 
-        lax.fori_loop(0, heads // pair, step, 0)
+        lax.fori_loop(0, groups, step, 0)
 
     def round_trip(c, _):
         wait_early(c)
@@ -199,6 +264,44 @@
     wait_late(last)
     finish(last, late_blocks, True)
 
+    start_all(read_copies())
+    landed[sp_place] = staged[sp_place]
+    reads[sp_place] = read[...]
+
+    for d, peer in enumerate(sp_peers):
+        pltpu.make_async_remote_copy(
+            src_ref=read, dst_ref=reads.at[peer], send_sem=read_send.at[d],
+            recv_sem=read_recv.at[peer], device_id={"sp": peer}, device_id_type=MESH,
+        ).wait_recv()
+        for g in range(groups):
+            piece = pl.ds(g * pair, pair)
+            pltpu.make_async_remote_copy(
+                src_ref=staged.at[peer, piece], dst_ref=landed.at[peer, piece],
+                send_sem=state_send.at[g, d], recv_sem=state_recv.at[g, peer],
+                device_id={"sp": peer}, device_id_type=MESH,
+            ).wait_recv()
+
+    row = lax.broadcasted_iota(jnp.int32, (SEQS, heads * vwidth), 0)
+    out = jnp.zeros((SEQS, heads * vwidth), F32)
+    for s in range(SEQS):
+        members = range(s * seq_span, (s + 1) * seq_span)
+        carried = functools.reduce(jnp.add, [reads[m] for m in members])
+        mixed = factor[...] * carried + own_term[s]
+        normed = mixed * lax.rsqrt(jnp.mean(mixed * mixed, axis=2, keepdims=True) + 1e-06)
+        line = jnp.concatenate([normed[h] for h in range(heads)], axis=1) * gain_ref[...]
+        out = jnp.where(row == s, jnp.broadcast_to(line, out.shape), out)
+        for h in range(heads):
+            cache_ref[s, h] = functools.reduce(
+                jnp.add, [landed[m, h].astype(F32) for m in members]
+            ).astype(BF16)
+    first_ref[...] = out.astype(BF16)
+
+    for copy in read_copies():
+        copy.wait_send()
+    for g in range(groups):
+        for copy in state_copies(g):
+            copy.wait_send()
+
     def drain(c, _):
         for copy in own_copies(c) + relay_copies(c):
             copy.wait_send()
@@ -207,14 +310,19 @@
     lax.fori_loop(0, chunks, drain, 0)
 
 
-def local_states(layer_input, key_weight, value_weight, decay_exponent, seq_span):
+def on_device(
+    layer_input, key_weight, value_weight, decay_exponent, query_new, key_new, value_new, norm_gain
+):
     tokens, feats = layer_input.shape
-    depth = key_weight.shape[0]
     parts = lax.axis_size("tp")
+    sp_size = lax.axis_size("sp")
+    seq_span = sp_size // SEQS
     side = math.isqrt(parts)
     heads = decay_exponent.shape[0]
     width = key_weight.shape[1] // heads
     vwidth = value_weight.shape[1] // heads
+    kept = width // sp_size
+    groups = heads // (2 if heads % 2 == 0 else 1)
     steps = np.linspace(0.0, 1.0, width // 2, dtype=np.float32)
     inverse = (np.float32(1.0) / np.power(np.float32(10000.0), steps)).astype(np.float32)
     inverse = jnp.asarray(np.concatenate([inverse, inverse])[None, :])
@@ -224,9 +332,12 @@
     rows = tokens // CHUNKS
     return pl.pallas_call(
         functools.partial(gather_kernel, side, seq_span, CHUNKS),
-        out_shape=jax.ShapeDtypeStruct((heads, width, vwidth), F32),
-        in_specs=[pl.BlockSpec(memory_space=pltpu.SMEM), vmem, anywhere, anywhere, anywhere],
-        out_specs=vmem,
+        out_shape=(
+            jax.ShapeDtypeStruct((SEQS, heads, kept, vwidth), BF16),
+            jax.ShapeDtypeStruct((SEQS, heads * vwidth), BF16),
+        ),
+        in_specs=[pl.BlockSpec(memory_space=pltpu.SMEM)] + [vmem] * 5 + [anywhere] * 3,
+        out_specs=(vmem, vmem),
         scratch_shapes=[
             pltpu.VMEM((parts, tokens, feats), BF16),
             pltpu.VMEM(key_weight.shape, BF16),
@@ -235,41 +346,29 @@
             pltpu.VMEM((tokens, width), F32),
             pltpu.VMEM((rows, heads * width), F32),
             pltpu.VMEM((rows, heads * vwidth), F32),
+            pltpu.VMEM((heads, width, vwidth), F32),
+            pltpu.VMEM((heads, width, vwidth), F32),
+            pltpu.VMEM((SEQS, heads, 1, vwidth), F32),
+            pltpu.VMEM((heads, 1, vwidth), F32),
+            pltpu.VMEM((sp_size, heads, kept, vwidth), BF16),
+            pltpu.VMEM((sp_size, heads, kept, vwidth), BF16),
+            pltpu.VMEM((heads, 1, vwidth), F32),
+            pltpu.VMEM((sp_size, heads, 1, vwidth), F32),
             pltpu.SemaphoreType.DMA((CHUNKS, sends)),
             pltpu.SemaphoreType.DMA((CHUNKS, parts, 2)),
             pltpu.SemaphoreType.DMA((3,)),
+            pltpu.SemaphoreType.DMA((groups, sp_size - 1)),
+            pltpu.SemaphoreType.DMA((groups, sp_size)),
+            pltpu.SemaphoreType.DMA((sp_size - 1,)),
+            pltpu.SemaphoreType.DMA((sp_size,)),
         ],
         compiler_params=pltpu.CompilerParams(
             collective_id=0, has_side_effects=True, vmem_limit_bytes=56 * 1024 * 1024
         ),
-    )(decay_exponent, inverse, layer_input, key_weight, value_weight)
-
-
-def on_device(
-    layer_input, key_weight, value_weight, decay_exponent, query_new, key_new, value_new, norm_gain
-):
-    head_local = decay_exponent.shape[0]
-    key_width = key_weight.shape[1] // head_local
-    value_width = value_weight.shape[1] // head_local
-    seq_span = lax.axis_size("sp") // SEQS
-    sp_place = lax.axis_index("sp")
-    local_state = local_states(layer_input, key_weight, value_weight, decay_exponent, seq_span)
-    member = (jnp.arange(SEQS, dtype=jnp.int32) == sp_place // seq_span).astype(jnp.float32)
-    state_terms = member[:, None, None, None] * local_state[None]
-    final_rows = lax.psum_scatter(state_terms, "sp", scatter_dimension=2, tiled=True)
-    state_cache = final_rows.astype(jnp.bfloat16)
-    queries = query_new.astype(jnp.float32).reshape(SEQS, head_local, key_width)
-    partial_read = jnp.einsum(
-        "shd,shde->she", queries, state_terms, precision=lax.Precision.HIGHEST
+    )(
+        decay_exponent, inverse, query_new, key_new, value_new, norm_gain.reshape(1, -1),
+        layer_input, key_weight, value_weight,
     )
-    carried = lax.psum(partial_read, "sp")
-    keys_next = key_new.astype(jnp.float32).reshape(SEQS, head_local, key_width)
-    values_next = value_new.astype(jnp.float32).reshape(SEQS, head_local, value_width)
-    own_term = jnp.sum(queries * keys_next, axis=2)[:, :, None] * values_next
-    mixed = jnp.exp(decay_exponent)[None, :, None] * carried + own_term
-    normed = mixed * lax.rsqrt(jnp.mean(mixed * mixed, axis=2, keepdims=True) + 1e-06)
-    normed = normed * norm_gain.reshape(head_local, value_width)[None, :, :]
-    return (state_cache, normed.reshape(SEQS, head_local * value_width).astype(jnp.bfloat16))
 
 
 def solution(mesh):

time: 135 us -> 94.5 us (0.70)
  waiting for transfers between devices: 15.5 us -> 0 us
  blocking collectives: 15 us -> 0 us
  between operations: 14.2 us -> 0.64 us
  Pallas kernels: 83.6 us -> 90.9 us
  other arithmetic: 4.01 us -> 0 us
  local copies, waits for them, and re-layouts: 0.65 us -> 2.75 us
  matrix products: 1.72 us -> 0 us
    reduce_scatter x1 -> x0, waiting for transfers between devices: 15.5 us -> none  [on_device(): lax.psum_scatter(state_terms, 'sp', scatter_dimension=2, tiled=True)]
    psum x1 -> x0, blocking collectives: 15 us -> none  [on_device(): carried = lax.psum(partial_read, 'sp')]
    pallas_call x1, Pallas kernels: 83.6 us -> 90.9 us  [on_device(): pl.pallas_call(functools.partial(gather_kernel, side, seq_span, CHUNKS),...]
    mul x2 -> x0, other arithmetic: 2.36 us -> none  [the longest x1 2.2 us: on_device(): state_terms = member[:, None, None, None] * local_state[None]]
    unnamed x11 -> x2, local copies, waits for them, and re-layouts: 0.64 us -> 2.75 us
    dot_general x1 -> x0, matrix products: 1.72 us -> none  [on_device(): jnp.einsum('shd,shde->she', queries, state_terms, precision=lax.Precision...]
    convert_element_type x2 -> x0, other arithmetic: 1.55 us -> none  [the longest x1 1.54 us: on_device(): state_cache = final_rows.astype(jnp.bfloat16)]
  transfers between devices with their start and end apart: 1 -> 0, of which waited for: 1 -> 0; matrix products, arithmetic and copies ran while one was open for 2% -> 0% of each run, Pallas kernels for 0% -> 0%
where the time goes in v2:
time: 94.5 us; the launch traced here: 94.3 us
  Pallas kernels  90.9 us (96%)
  local copies, waits for them, and re-layouts  2.75 us (3%)
    pallas_call x1, Pallas kernels, on_device(): pl.pallas_call(functools.partial(gather_kernel, side, seq_span, CHUNKS),...  90.9 us
    unnamed x2, local copies, waits for them, and re-layouts  2.75 us

profile of v2, /device:TPU:0, one launch (start us, length us, event | category | flops | bytes accessed | tf_op | source)
XLA Modules:
  0.0 94.3 jit_solution(2680478453536503005)
XLA Ops:
  0.6 90.9 %shard_map.104 = (bf16[2,8,16,128]{3,2,1,0:T(8,128)(2,1)}, bf16[2,1024]{1,0:T(2,128)(2,1)}) custom-call(f32[8]{0:T(128)} %decay_ref.1, f32[1,128]{1,0:T(1,128)} %constant.2.clone.inv_ref, bf16[2,1024]{1,0:T(2,128)(2,1)} %query_ref.1, bf16[2,1024]{1,0:T(2,128)(2,1)} %key_ref.1, bf16[2,1024]{1,0:T(2,128)(2,1)} %value_ref.1, f32[1,1024]{1,0:T(1,128)} %bitcast.1, ...), custom_call_target="tpu_custom_call" | custom-call | tf_op jit(solution)/shard_map/pallas_call | solution.py:333
  91.5 1.5 %copy.13 = bf16[2,8,16,128]{3,2,1,0:T(8,128)(2,1)} copy(bf16[2,8,16,128]{3,2,1,0:T(8,128)(2,1)} %get-tuple-element.4) | data formatting | bytes 131072
  93.0 1.3 %copy.14 = bf16[2,1024]{1,0:T(2,128)(2,1)} copy(bf16[2,1024]{1,0:T(2,128)(2,1)} %get-tuple-element.5) | data formatting | bytes 8192

commit v3 on v2

--- a/solution.py
+++ b/solution.py
@@ -10,7 +10,7 @@
 from jax.sharding import PartitionSpec as P
 
 SEQS = 2
-CHUNKS = 4
+CHUNKS = 8
 MESH = pl.DeviceIdType.MESH
 F32 = jnp.float32
 BF16 = jnp.bfloat16
@@ -18,8 +18,9 @@
 
 def gather_kernel(
     side, seq_span, chunks,
-    decay_ref, inv_ref, query_ref, key_ref, value_ref, gain_ref, x_ref, wk_ref, wv_ref,
+    decay_hbm, inv_hbm, query_hbm, key_hbm, value_hbm, gain_hbm, x_ref, wk_ref, wv_ref,
     cache_ref, first_ref,
+    decay_ref, inv_ref, query_ref, key_ref, value_ref, gain_ref,
     gx, wk, wv, cosine, sine, acc_k, acc_v,
     state_ref, query_wide, own_term, factor, staged, landed, read, reads,
     send_sem, recv_sem, local_sem, state_send, state_recv, read_send, read_recv,
@@ -46,14 +47,6 @@
     x_peers = [x_peer(d) for d in range(1, side)]
     y_peers = [y_peer(d) for d in range(1, side)]
 
-    local = [
-        pltpu.make_async_copy(x_ref, gx.at[me], local_sem.at[0]),
-        pltpu.make_async_copy(wk_ref, wk, local_sem.at[1]),
-        pltpu.make_async_copy(wv_ref, wv, local_sem.at[2]),
-    ]
-    for copy in local:
-        copy.start()
-
     barrier = pltpu.get_barrier_semaphore()
     for peer in x_peers + y_peers:
         pl.semaphore_signal(barrier, inc=1, device_id={"tp": peer}, device_id_type=MESH)
@@ -120,7 +113,25 @@
     if chunks > 1:
         start_all(own_copies(1))
 
+    small = [
+        pltpu.make_async_copy(source, target, local_sem.at[3 + i])
+        for i, (source, target) in enumerate((
+            (decay_hbm, decay_ref), (inv_hbm, inv_ref), (query_hbm, query_ref),
+            (key_hbm, key_ref), (value_hbm, value_ref), (gain_hbm, gain_ref),
+        ))
+    ]
+    for copy in small:
+        copy.start()
+    local = [
+        pltpu.make_async_copy(x_ref, gx.at[me], local_sem.at[0]),
+        pltpu.make_async_copy(wk_ref, wk, local_sem.at[1]),
+        pltpu.make_async_copy(wv_ref, wv, local_sem.at[2]),
+    ]
+    for copy in local:
+        copy.start()
     state_ref[...] = jnp.zeros_like(state_ref)
+    for copy in small:
+        copy.wait()
     base = lax.rem(sp_place, seq_span) * tokens
 
     def table(c, _):
@@ -310,6 +321,11 @@
     lax.fori_loop(0, chunks, drain, 0)
 
 
+def settle(cache_ref, first_ref, cache_out, first_out):
+    cache_out[...] = cache_ref[...]
+    first_out[...] = first_ref[...]
+
+
 def on_device(
     layer_input, key_weight, value_weight, decay_exponent, query_new, key_new, value_new, norm_gain
 ):
@@ -330,15 +346,21 @@
     anywhere = pl.BlockSpec(memory_space=pl.ANY)
     vmem = pl.BlockSpec(memory_space=pltpu.VMEM)
     rows = tokens // CHUNKS
-    return pl.pallas_call(
+    state_cache, first_read = pl.pallas_call(
         functools.partial(gather_kernel, side, seq_span, CHUNKS),
         out_shape=(
             jax.ShapeDtypeStruct((SEQS, heads, kept, vwidth), BF16),
             jax.ShapeDtypeStruct((SEQS, heads * vwidth), BF16),
         ),
-        in_specs=[pl.BlockSpec(memory_space=pltpu.SMEM)] + [vmem] * 5 + [anywhere] * 3,
+        in_specs=[anywhere] * 9,
         out_specs=(vmem, vmem),
         scratch_shapes=[
+            pltpu.SMEM((heads,), F32),
+            pltpu.VMEM(inverse.shape, F32),
+            pltpu.VMEM(query_new.shape, BF16),
+            pltpu.VMEM(key_new.shape, BF16),
+            pltpu.VMEM(value_new.shape, BF16),
+            pltpu.VMEM((1, heads * vwidth), F32),
             pltpu.VMEM((parts, tokens, feats), BF16),
             pltpu.VMEM(key_weight.shape, BF16),
             pltpu.VMEM(value_weight.shape, BF16),
@@ -356,19 +378,28 @@
             pltpu.VMEM((sp_size, heads, 1, vwidth), F32),
             pltpu.SemaphoreType.DMA((CHUNKS, sends)),
             pltpu.SemaphoreType.DMA((CHUNKS, parts, 2)),
-            pltpu.SemaphoreType.DMA((3,)),
+            pltpu.SemaphoreType.DMA((9,)),
             pltpu.SemaphoreType.DMA((groups, sp_size - 1)),
             pltpu.SemaphoreType.DMA((groups, sp_size)),
             pltpu.SemaphoreType.DMA((sp_size - 1,)),
             pltpu.SemaphoreType.DMA((sp_size,)),
         ],
         compiler_params=pltpu.CompilerParams(
-            collective_id=0, has_side_effects=True, vmem_limit_bytes=56 * 1024 * 1024
+            collective_id=0, has_side_effects=True, vmem_limit_bytes=62 * 1024 * 1024
         ),
     )(
         decay_exponent, inverse, query_new, key_new, value_new, norm_gain.reshape(1, -1),
         layer_input, key_weight, value_weight,
     )
+    return pl.pallas_call(
+        settle,
+        out_shape=(
+            jax.ShapeDtypeStruct(state_cache.shape, BF16),
+            jax.ShapeDtypeStruct(first_read.shape, BF16),
+        ),
+        in_specs=[vmem, vmem],
+        out_specs=(vmem, vmem),
+    )(state_cache, first_read)
 
 
 def solution(mesh):

time: 94.5 us -> 91.7 us (0.970)
  local copies, waits for them, and re-layouts: 2.75 us -> 0 us
    unnamed x2 -> x0, local copies, waits for them, and re-layouts: 2.75 us -> none
    pallas_call x1, Pallas kernels: 90.9 us -> 89.4 us  [on_device(): pl.pallas_call(functools.partial(gather_kernel, side, seq_span, CHUNKS),...]
    pallas_call x0 -> x1, Pallas kernels: none -> 1.48 us  [on_device(): pl.pallas_call(settle, out_shape=(jax.ShapeDtypeStruct(state_cache.shape,...]
where the time goes in v3:
time: 91.7 us; the launch traced here: 91.5 us
  Pallas kernels  90.9 us (99%)
    pallas_call x1, Pallas kernels, on_device(): pl.pallas_call(functools.partial(gather_kernel, side, seq_span, CHUNKS),...  89.4 us

profile of v3, /device:TPU:0, one launch (start us, length us, event | category | flops | bytes accessed | tf_op | source)
XLA Modules:
  0.0 91.5 jit_solution(16338447147243888025)
XLA Ops:
  0.6 89.4 %shard_map.104 = (bf16[2,8,16,128]{3,2,1,0:T(8,128)(2,1)}, bf16[2,1024]{1,0:T(2,128)(2,1)}) custom-call(f32[8]{0:T(128)} %decay_hbm.1, f32[1,128]{1,0:T(1,128)} %constant.2.clone.inv_hbm, bf16[2,1024]{1,0:T(2,128)(2,1)} %query_hbm.1, bf16[2,1024]{1,0:T(2,128)(2,1)} %key_hbm.1, bf16[2,1024]{1,0:T(2,128)(2,1)} %value_hbm.1, f32[1,1024]{1,0:T(1,128)} %bitcast.1, ...), custom_call_target="tpu_custom_call" | custom-call | tf_op jit(solution)/shard_map/pallas_call | solution.py:349
  90.0 1.5 %shard_map.105 = (bf16[2,8,16,128]{3,2,1,0:T(8,128)(2,1)}, bf16[2,1024]{1,0:T(2,128)(2,1)}) custom-call(bf16[2,8,16,128]{3,2,1,0:T(8,128)(2,1)} %get-tuple-element.4.cache_ref, bf16[2,1024]{1,0:T(2,128)(2,1)} %get-tuple-element.5.first_ref), custom_call_target="tpu_custom_call" | custom-call | tf_op jit(solution)/shard_map/pallas_call | solution.py:394

commit v4 on v3

--- a/solution.py
+++ b/solution.py
@@ -29,7 +29,7 @@
     rows = tokens // chunks
     half = rows // 2
     heads, width, vwidth = state_ref.shape
-    pair = 2 if heads % 2 == 0 else 1
+    pair = next(p for p in (4, 2, 1) if heads % p == 0)
     me = lax.axis_index("tp")
     my_y, my_x = me // side, lax.rem(me, side)
     sp_place = lax.axis_index("sp")
@@ -338,7 +338,7 @@
     width = key_weight.shape[1] // heads
     vwidth = value_weight.shape[1] // heads
     kept = width // sp_size
-    groups = heads // (2 if heads % 2 == 0 else 1)
+    groups = heads // next(p for p in (4, 2, 1) if heads % p == 0)
     steps = np.linspace(0.0, 1.0, width // 2, dtype=np.float32)
     inverse = (np.float32(1.0) / np.power(np.float32(10000.0), steps)).astype(np.float32)
     inverse = jnp.asarray(np.concatenate([inverse, inverse])[None, :])

time: 91.7 us -> 89.7 us (0.978)
  Pallas kernels: 90.9 us -> 88.9 us
    pallas_call x1, Pallas kernels: 89.4 us -> 87.4 us  [on_device(): pl.pallas_call(functools.partial(gather_kernel, side, seq_span, CHUNKS),...]
where the time goes in v4:
time: 89.7 us; the launch traced here: 89.5 us
  Pallas kernels  88.9 us (99%)
    pallas_call x1, Pallas kernels, on_device(): pl.pallas_call(functools.partial(gather_kernel, side, seq_span, CHUNKS),...  87.4 us

profile of v4, /device:TPU:0, one launch (start us, length us, event | category | flops | bytes accessed | tf_op | source)
XLA Modules:
  0.0 89.5 jit_solution(5855808058012538349)
XLA Ops:
  0.6 87.4 %shard_map.104 = (bf16[2,8,16,128]{3,2,1,0:T(8,128)(2,1)}, bf16[2,1024]{1,0:T(2,128)(2,1)}) custom-call(f32[8]{0:T(128)} %decay_hbm.1, f32[1,128]{1,0:T(1,128)} %constant.2.clone.inv_hbm, bf16[2,1024]{1,0:T(2,128)(2,1)} %query_hbm.1, bf16[2,1024]{1,0:T(2,128)(2,1)} %key_hbm.1, bf16[2,1024]{1,0:T(2,128)(2,1)} %value_hbm.1, f32[1,1024]{1,0:T(1,128)} %bitcast.1, ...), custom_call_target="tpu_custom_call" | custom-call | tf_op jit(solution)/shard_map/pallas_call | solution.py:349
  88.0 1.5 %shard_map.105 = (bf16[2,8,16,128]{3,2,1,0:T(8,128)(2,1)}, bf16[2,1024]{1,0:T(2,128)(2,1)}) custom-call(bf16[2,8,16,128]{3,2,1,0:T(8,128)(2,1)} %get-tuple-element.4.cache_ref, bf16[2,1024]{1,0:T(2,128)(2,1)} %get-tuple-element.5.first_ref), custom_call_target="tpu_custom_call" | custom-call | tf_op jit(solution)/shard_map/pallas_call | solution.py:394
